TPU v7x, 32 devices: a whole 2x2x4 slice. The times are simulated.
32 devices in a mesh: sp: 16 (over z, y, x), tp: 2 (over core).
Axes of the slice: x: 2, y: 2, z: 4, core: 2. Of those that a mesh axis runs over, the one named last changes fastest.
Arguments:
- query: bfloat16 [2048, 2048], P('sp', 'tp'), may hold values from -6 to 6
- forget_logit: bfloat16 [2048, 2048], P('sp', 'tp'), may hold values from -7.5 to 7.5
- value: bfloat16 [2048, 2048], P('sp', 'tp'), may hold values from -6 to 6
- out_gate: bfloat16 [2048, 2048], P('sp', 'tp'), may hold values from -6 to 6
- lower_bound: float32 [2048], P('tp'), may hold values from 0.9 to 1, as said below
- head_gain: float32 [2048], P('tp'), may hold values from 0.1 to 1.9
- residual_in: bfloat16 [2048, 2048], P(('sp', 'tp')), may hold values from -6 to 6
- w_out: bfloat16 [2048, 2048], replicated, may hold values from -0.125 to 0.125
- ffn_gain: float32 [2048], replicated, may hold values from 0.1 to 1.9
- routing: int32 [2048, 2], P(('sp', 'tp')), may hold values from 0 to 15, all different within a row; in each aligned block of 64 rows (0 to 63, 64 to 127, ...) at most 16 rows name the same one
- route_weight: float32 [2048, 2], P(('sp', 'tp')), may hold values from 0.25 to 1
- expert_gate: bfloat16 [16, 2048, 1024], P('sp', None, 'tp'), may hold values from -0.125 to 0.125
- expert_up: bfloat16 [16, 2048, 1024], P('sp', None, 'tp'), may hold values from -0.125 to 0.125
- expert_down: bfloat16 [16, 1024, 2048], P('sp', 'tp'), may hold values from -0.1875 to 0.1875
Outputs:
- layer_out: bfloat16 [2048, 2048], P(('sp', 'tp'))
Inputs may be any that keep to these rules, and one draw needn't show every extreme that they name: `routing`: each row names 2 different experts. In each aligned block of 64 rows (the rows of one device) no expert is named by more than 16 rows, a bound that some blocks reach. 1 - lower_bound is at least 1 / 4096.
All inputs are finite; a program needn't handle non-finite values.
Results may differ from a plain program's by a relative error of at most 0.012.
Values may be sent and summed in bfloat16 or wider, within the bound.
A program may use at most 128 MiB of HBM per device.

v0:
```python
import functools

import jax
import jax.numpy as jnp
from jax import lax
from jax.experimental import pallas as pl
from jax.experimental.pallas import tpu as pltpu
from jax.sharding import PartitionSpec as P

HEAD_DIM = 128
MESH = pl.DeviceIdType.MESH
epsilon = 1e-06
f32 = jnp.float32
bf16 = jnp.bfloat16
NT = (((1,), (1,)), ((), ()))
TN = (((0,), (0,)), ((), ()))


def dot(a, b, dims=(((1,), (0,)), ((), ())), precision=None):
    return lax.dot_general(a, b, dims, precision=precision, preferred_element_type=f32)


def rows_of(index, count):
    return pl.ds(pl.multiple_of(index * count, count), count)


def greet(n):
    me, core = lax.axis_index("sp"), lax.axis_index("tp")
    barrier = pltpu.get_barrier_semaphore()
    pl.semaphore_signal(barrier, inc=1, device_id={"tp": 1 - core}, device_id_type=MESH)

    @pl.loop(1, n)
    def _(r):
        pl.semaphore_signal(
            barrier, inc=1, device_id={"sp": lax.rem(me + r, n)}, device_id_type=MESH
        )

    return barrier


def partner(me, r):
    other = me
    step = 1
    while step <= r:
        if r & step:
            other = other + step * (1 - 2 * (me // step % 2))
        step *= 2
    return other


def layer_kernel(
    n, cap,
    query_h, logit_h, value_h, gate_h, bound_h, gain_h, residual_h, ffn_gain_h, routing_h,
    weight_h, w_hbm, g_hbm, u_hbm, d_hbm,
    layer_out,
    query, logit, value, gate, bound, gain, residual, ffn_gain, routing, weight,
    w_out, q_scr, k_scr, ho, st_send, st_recv, dec_send, dec_recv, ret_send, ret_recv,
    mixed, regrouped, proj,
    wg, wu, wd, outbox, arrived, hidden, result, returned,
    in_sem, w_sem, s_sem, r_sem, ds_sem, dr_sem, bs_sem, br_sem, ms_sem, mr_sem,
    l_sem, ps_sem, pr_sem, xs_sem, xr_sem, ys_sem, yr_sem,
):
    me, core = lax.axis_index("sp"), lax.axis_index("tp")
    length, width = query.shape
    heads = width // HEAD_DIM
    groups, piece = st_recv.shape[0], st_recv.shape[2]
    per = heads // groups
    half = length // 2
    moves = [
        pltpu.make_async_copy(src, dst, in_sem.at[i])
        for i, (src, dst) in enumerate((
            (logit_h, logit), (bound_h, bound), (query_h, query), (value_h, value),
            (routing_h, routing), (weight_h, weight), (gate_h, gate), (gain_h, gain),
            (residual_h, residual), (ffn_gain_h, ffn_gain),
        ))
    ]
    for move in moves:
        move.start()
    barrier = greet(n)
    w_copy = pltpu.make_async_copy(w_hbm, w_out, w_sem)
    homes = ((g_hbm, wg), (u_hbm, wu), (d_hbm, wd))
    local = [
        pltpu.make_async_copy(src.at[0], dst.at[0], l_sem.at[i])
        for i, (src, dst) in enumerate(homes)
    ]
    peer = [
        pltpu.make_async_remote_copy(
            src_ref=src.at[0], dst_ref=dst.at[1],
            send_sem=ps_sem.at[i], recv_sem=pr_sem.at[i],
            device_id={"tp": 1 - core}, device_id_type=MESH,
        )
        for i, (src, dst) in enumerate(homes)
    ]
    for move in moves[:4]:
        move.wait()
    w_copy.start()

    row = lax.broadcasted_iota(jnp.int32, (length, length), 0)
    col = lax.broadcasted_iota(jnp.int32, (length, length), 1)
    causal = row >= col
    tri = causal.astype(f32)
    def owned(g, index):
        return pl.ds(pl.multiple_of(g * per * HEAD_DIM + index * piece, piece), piece)

    def state_copy(g, r):
        return pltpu.make_async_remote_copy(
            src_ref=st_send.at[owned(g, partner(me, r))], dst_ref=st_recv.at[g, r],
            send_sem=s_sem.at[g, r], recv_sem=r_sem.at[g, r],
            device_id={"sp": partner(me, r)}, device_id_type=MESH,
        )

    def decay_copy(g, r):
        return pltpu.make_async_remote_copy(
            src_ref=dec_send.at[g], dst_ref=dec_recv.at[g, r],
            send_sem=ds_sem.at[g, r], recv_sem=dr_sem.at[g, r],
            device_id={"sp": partner(me, r)}, device_id_type=MESH,
        )

    def back_copy(g, r):
        return pltpu.make_async_remote_copy(
            src_ref=ret_send.at[g, partner(me, r)], dst_ref=ret_recv.at[owned(g, me)],
            send_sem=bs_sem.at[g, r], recv_sem=br_sem.at[g, r],
            device_id={"sp": partner(me, r)}, device_id_type=MESH,
        )

    def back_from(g, r):
        return pltpu.make_async_remote_copy(
            src_ref=ret_send.at[g, me], dst_ref=ret_recv.at[owned(g, partner(me, r))],
            send_sem=bs_sem.at[g, r], recv_sem=br_sem.at[g, r],
            device_id={"sp": partner(me, r)}, device_id_type=MESH,
        )

    others = range(n - 1, 0, -1)

    for h in range(heads):
        c = slice(h * HEAD_DIM, (h + 1) * HEAD_DIM)
        key = (1.0 - bound[:, c]) / (1.0 + jnp.exp(logit[:, c].astype(f32)))
        cum = dot(tri, jnp.log1p(-key), precision=lax.Precision.HIGHEST)
        last = cum[length - 1 :, :]
        mid = 0.5 * last
        q_scr[:, c] = (query[:, c].astype(f32) * jnp.exp(cum - mid)).astype(bf16)
        keys = (key * jnp.exp(mid - cum)).astype(bf16)
        k_scr[:, c] = keys
        st_send[c, :] = (dot(value[:, c], keys, TN) * jnp.exp(mid)).astype(bf16)
        g = h // per
        dec_send[g, h % per : h % per + 1, :] = last
        if h == 0:
            pl.semaphore_wait(barrier, n)
        if h % per == per - 1:
            for r in others:
                decay_copy(g, r).start()
                state_copy(g, r).start()
            st_recv[g, 0] = st_send[owned(g, me), :]
            dec_recv[g, 0] = dec_send[g]
            if g == 0:
                for copy in peer + local:
                    copy.start()

    for h in range(heads):
        c = slice(h * HEAD_DIM, (h + 1) * HEAD_DIM)
        scores = jnp.where(causal, dot(q_scr[:, c], k_scr[:, c], NT), 0.0).astype(bf16)
        ho[:, c] = dot(scores, value[:, c])

    slots = n * cap
    for move in moves[4:]:
        move.wait()
    top, count = routing.shape
    eye = lax.broadcasted_iota(jnp.int32, (count, count), 0) == lax.broadcasted_iota(
        jnp.int32, (count, count), 1
    )

    def column(line):
        return jnp.sum(jnp.where(eye, line, 0.0), axis=1, keepdims=True)

    expert = lax.broadcasted_iota(jnp.int32, (count, n), 1).astype(f32)
    slot_of = lax.broadcasted_iota(jnp.int32, (count, slots), 1)
    before = (
        lax.broadcasted_iota(jnp.int32, (count, count), 0)
        > lax.broadcasted_iota(jnp.int32, (count, count), 1)
    ).astype(bf16)
    used = jnp.zeros((1, n), f32)
    picks = jnp.zeros((count, slots), f32)
    combine = jnp.zeros((count, slots), f32)
    for k in range(top):
        hot = (column(routing[k : k + 1, :].astype(f32)) == expert).astype(f32)
        rank = dot(before, hot.astype(bf16)) + used
        used = used + jnp.sum(hot, axis=0, keepdims=True)
        slot = jnp.sum(hot * (rank + expert * cap), axis=1, keepdims=True)
        mine = slot.astype(jnp.int32) == slot_of
        picks = jnp.where(mine, 1.0, picks)
        combine = jnp.where(mine, column(weight[k : k + 1, :]), combine)
    high = combine.astype(bf16)
    both = jnp.concatenate([high, (combine - high.astype(f32)).astype(bf16)], axis=0)

    for g in range(groups):
        for r in others:
            decay_copy(g, r).wait_recv()
            state_copy(g, r).wait_recv()
        own_head = me * piece // HEAD_DIM

        def prefix(p, acc):
            r = 0
            step = 1
            while step < n:
                r = r + step * ((me // step + p // step) % 2)
                step *= 2
            last = dec_recv[g, r, pl.ds(own_head, 1), :]
            ret_send[g, p] = (acc * jnp.exp(0.5 * last)).astype(bf16)
            return acc * jnp.exp(last) + st_recv[g, r].astype(f32)

        lax.fori_loop(0, n, prefix, jnp.zeros((piece, HEAD_DIM), f32))
        for r in others:
            back_copy(g, r).start()
        ret_recv[owned(g, me), :] = ret_send[g, me]

    for h in range(heads):
        c = slice(h * HEAD_DIM, (h + 1) * HEAD_DIM)
        if h % per == 0:
            for r in others:
                back_from(h // per, r).wait_recv()
        out = ho[:, c] + dot(q_scr[:, c], ret_recv[c, :], NT)
        out = out * lax.rsqrt(jnp.mean(out * out, axis=1, keepdims=True) + epsilon)
        g = gate[:, c].astype(f32)
        out = (out * gain[:, c] * (g / (1.0 + jnp.exp(-g)))).astype(bf16)
        mixed[0, :, c] = out[:half]
        mixed[1, :, c] = out[half:]

    swap = pltpu.make_async_remote_copy(
        src_ref=mixed.at[1 - core], dst_ref=regrouped,
        send_sem=ms_sem, recv_sem=mr_sem,
        device_id={"tp": 1 - core}, device_id_type=MESH,
    )
    swap.start()
    w_copy.wait()
    tile = 512
    total = w_out.shape[1]

    def project(which, source, first):
        @pl.loop(0, total // tile)
        def _(j):
            cols = pl.ds(pl.multiple_of(j * tile, tile), tile)
            part = dot(source, w_out[rows_of(which, width), cols])
            proj[:, cols] = part if first else proj[:, cols] + part

    project(core, mixed[core], True)
    swap.wait()
    project(1 - core, regrouped[...], False)
    updated = (residual[...].astype(f32) + proj[...]).astype(bf16)
    updated = updated.astype(f32)
    proj[...] = updated
    normed = (
        updated
        * lax.rsqrt(jnp.mean(updated * updated, axis=1, keepdims=True) + epsilon)
        * ffn_gain[...]
    ).astype(bf16)
    outbox[...] = dot(picks.astype(bf16), normed, TN).astype(bf16)

    sets = [
        [r for r in range(n - 1, -1, -1) if (r ^ (r >> 1)) & 1 == which] for which in range(2)
    ]
    place = {r: i for i, r in enumerate(sets[0] + sets[1])}

    def block(r):
        return pl.ds(place[r] * cap, cap)

    def send_copy(r):
        return pltpu.make_async_remote_copy(
            src_ref=outbox.at[rows_of(partner(me, r), cap)], dst_ref=arrived.at[block(r)],
            send_sem=xs_sem.at[r], recv_sem=xr_sem.at[r],
            device_id={"sp": partner(me, r)}, device_id_type=MESH,
        )

    def answer_copy(r):
        return pltpu.make_async_remote_copy(
            src_ref=result.at[block(r)], dst_ref=returned.at[rows_of(me, cap)],
            send_sem=ys_sem.at[r], recv_sem=yr_sem.at[r],
            device_id={"sp": partner(me, r)}, device_id_type=MESH,
        )

    def answer_from(r):
        return pltpu.make_async_remote_copy(
            src_ref=result.at[block(r)], dst_ref=returned.at[rows_of(partner(me, r), cap)],
            send_sem=ys_sem.at[r], recv_sem=yr_sem.at[r],
            device_id={"sp": partner(me, r)}, device_id_type=MESH,
        )

    for r in sets[0] + sets[1]:
        if r:
            send_copy(r).start()
    arrived[block(0), :] = outbox[rows_of(me, cap), :]
    for copy in peer + local:
        copy.wait()
    inner = wg.shape[2]
    narrow = 256
    first = 0
    for group in sets:
        for r in group:
            if r:
                send_copy(r).wait_recv()
        part = slice(first, first + len(group) * cap)
        first = first + len(group) * cap
        for s in range(2):

            @pl.loop(0, inner // narrow)
            def _(j):
                cols = rows_of(j, narrow)
                g = dot(arrived[part, :], wg[s, :, cols])
                u = dot(arrived[part, :], wu[s, :, cols])
                hidden[s, part, cols] = (g / (1.0 + jnp.exp(-g)) * u).astype(bf16)

        @pl.loop(0, total // tile)
        def _(j):
            cols = rows_of(j, tile)
            result[part, cols] = (
                dot(hidden[0, part, :], wd[0, :, cols]) + dot(hidden[1, part, :], wd[1, :, cols])
            ).astype(bf16)

        for r in group:
            if r:
                answer_copy(r).start()

    returned[rows_of(me, cap), :] = result[block(0), :]
    for r in sets[0] + sets[1]:
        if r:
            answer_from(r).wait_recv()

    @pl.loop(0, total // tile)
    def _(j):
        cols = rows_of(j, tile)
        back = dot(both, returned[:, cols])
        layer_out[:, cols] = (proj[:, cols] + (back[:count] + back[count:])).astype(bf16)

    for g in range(groups):
        for r in others:
            decay_copy(g, r).wait_send()
            state_copy(g, r).wait_send()
            back_copy(g, r).wait_send()

    for r in range(1, n):
        send_copy(r).wait_send()
        answer_copy(r).wait_send()


def solution(mesh):
    n = mesh.shape["sp"]
    vmem = pl.BlockSpec(memory_space=pltpu.VMEM)
    hbm = pl.BlockSpec(memory_space=pl.ANY)
    dma = pltpu.SemaphoreType.DMA

    def body(
        query, forget_logit, value, out_gate, lower_bound, head_gain, residual_in, w_out,
        ffn_gain, routing, route_weight, expert_gate, expert_up, expert_down,
    ):
        length, width = query.shape
        heads = width // HEAD_DIM
        half, model = residual_in.shape
        cap = 2 * half * routing.shape[1] // n
        cap = -(-cap // 16) * 16
        slots = n * cap
        groups = 2 if heads % 2 == 0 and width // n % 32 == 0 else 1
        piece = width // n // groups
        inner = expert_gate.shape[2]
        top = routing.shape[1]
        return pl.pallas_call(
            functools.partial(layer_kernel, n, cap),
            out_shape=jax.ShapeDtypeStruct((half, model), bf16),
            in_specs=[hbm] * 14,
            out_specs=vmem,
            scratch_shapes=[
                pltpu.VMEM((length, width), bf16),
                pltpu.VMEM((length, width), bf16),
                pltpu.VMEM((length, width), bf16),
                pltpu.VMEM((length, width), bf16),
                pltpu.VMEM((1, width), f32),
                pltpu.VMEM((1, width), f32),
                pltpu.VMEM((half, model), bf16),
                pltpu.VMEM((1, model), f32),
                pltpu.VMEM((top, half), jnp.int32),
                pltpu.VMEM((top, half), f32),
                pltpu.VMEM(w_out.shape, bf16),
                pltpu.VMEM((length, width), bf16),
                pltpu.VMEM((length, width), bf16),
                pltpu.VMEM((length, width), f32),
                pltpu.VMEM((width, HEAD_DIM), bf16),
                pltpu.VMEM((groups, n, piece, HEAD_DIM), bf16),
                pltpu.VMEM((groups, heads // groups, HEAD_DIM), f32),
                pltpu.VMEM((groups, n, heads // groups, HEAD_DIM), f32),
                pltpu.VMEM((groups, n, piece, HEAD_DIM), bf16),
                pltpu.VMEM((width, HEAD_DIM), bf16),
                pltpu.VMEM((2, half, width), bf16),
                pltpu.VMEM((half, width), bf16),
                pltpu.VMEM((half, model), f32),
                pltpu.VMEM((2, model, inner), bf16),
                pltpu.VMEM((2, model, inner), bf16),
                pltpu.VMEM((2, inner, model), bf16),
                pltpu.VMEM((slots, model), bf16),
                pltpu.VMEM((slots, model), bf16),
                pltpu.VMEM((2, slots, inner), bf16),
                pltpu.VMEM((slots, model), bf16),
                pltpu.VMEM((slots, model), bf16),
                dma((10,)), dma,
                dma((groups, n)), dma((groups, n)), dma((groups, n)),
                dma((groups, n)), dma((groups, n)), dma((groups, n)),
                dma, dma, dma((3,)), dma((3,)), dma((3,)),
                dma((n,)), dma((n,)), dma((n,)), dma((n,)),
            ],
            compiler_params=pltpu.CompilerParams(
                collective_id=0, has_side_effects=True, vmem_limit_bytes=60 << 20
            ),
        )(
            query, forget_logit, value, out_gate, lower_bound[None], head_gain[None],
            residual_in, ffn_gain[None], routing.T, route_weight.T, w_out,
            expert_gate, expert_up, expert_down,
        )

    placed = (
        P("sp", "tp"), P("sp", "tp"), P("sp", "tp"), P("sp", "tp"), P("tp"), P("tp"),
        P(("sp", "tp"), None), P(), P(), P(("sp", "tp"), None), P(("sp", "tp"), None),
        P("sp", None, "tp"), P("sp", None, "tp"), P("sp", "tp", None),
    )
    return jax.shard_map(
        body, mesh=mesh, in_specs=placed, out_specs=P(("sp", "tp"), None), check_vma=False
    )
```

profile of v0, /device:TPU:0, one launch (start us, length us, event | category | flops | bytes accessed | tf_op | source)
XLA Modules:
  0.0 79.3 jit_solution(12146962437638094104)
XLA Ops:
  0.0 77.7 %shard_map.136 = bf16[64,2048]{1,0:T(8,128)(2,1)} custom-call(bf16[128,1024]{1,0:T(8,128)(2,1)} %query_h.1, bf16[128,1024]{1,0:T(8,128)(2,1)} %logit_h.1, bf16[128,1024]{1,0:T(8,128)(2,1)} %value_h.1, bf16[128,1024]{1,0:T(8,128)(2,1)} %gate_h.1, f32[1,1024]{1,0:T(1,128)} %bitcast.6, f32[1,1024]{1,0:T(1,128)} %bitcast.7, bf16[64,2048]{1,0:T(8,128)(2,1)} %residual_h.1, ...), custom_call_target="tpu_custom_call" | custom-call | tf_op jit(solution)/shard_map/pallas_call | solution.py:364
  77.7 1.7 %copy.16 = bf16[64,2048]{1,0:T(8,128)(2,1)} copy(bf16[64,2048]{1,0:T(8,128)(2,1)} %shard_map.136) | data formatting | bytes 524288
where the time goes:
time: 79.5 us; the launch traced here: 79.3 us
  Pallas kernels  77.7 us (98%)
  local copies, waits for them, and re-layouts  1.67 us (2%)
    pallas_call x1, Pallas kernels, body(): pl.pallas_call(functools.partial(layer_kernel, n, cap), out_shape=jax.Sha...  77.7 us
    unnamed x1, local copies, waits for them, and re-layouts  1.67 us

commit v1 on v0

--- a/solution.py
+++ b/solution.py
@@ -56,9 +56,11 @@
     query, logit, value, gate, bound, gain, residual, ffn_gain, routing, weight,
     w_out, q_scr, k_scr, ho, st_send, st_recv, dec_send, dec_recv, ret_send, ret_recv,
     mixed, regrouped, proj,
-    wg, wu, wd, outbox, arrived, hidden, result, returned,
+    wg, wu, wd, gated, normed, pick, comb, info_send, info_recv,
+    outbox, arrived, hidden, result, returned, dense_in, relay_out, relay_in, dense_out, dense_ret,
     in_sem, w_sem, s_sem, r_sem, ds_sem, dr_sem, bs_sem, br_sem, ms_sem, mr_sem,
-    l_sem, ps_sem, pr_sem, xs_sem, xr_sem, ys_sem, yr_sem,
+    l_sem, ps_sem, pr_sem, is_sem, ir_sem, xs_sem, xr_sem, ys_sem, yr_sem,
+    vs_sem, vr_sem, fs_sem, fr_sem, gs_sem, gr_sem, es_sem, er_sem,
 ):
     me, core = lax.axis_index("sp"), lax.axis_index("tp")
     length, width = query.shape
@@ -91,9 +93,11 @@
         )
         for i, (src, dst) in enumerate(homes)
     ]
+    w_copy.start()
+    for copy in local:
+        copy.start()
     for move in moves[:4]:
         move.wait()
-    w_copy.start()
 
     row = lax.broadcasted_iota(jnp.int32, (length, length), 0)
     col = lax.broadcasted_iota(jnp.int32, (length, length), 1)
@@ -137,66 +141,107 @@
         key = (1.0 - bound[:, c]) / (1.0 + jnp.exp(logit[:, c].astype(f32)))
         cum = dot(tri, jnp.log1p(-key), precision=lax.Precision.HIGHEST)
         last = cum[length - 1 :, :]
-        mid = 0.5 * last
-        q_scr[:, c] = (query[:, c].astype(f32) * jnp.exp(cum - mid)).astype(bf16)
-        keys = (key * jnp.exp(mid - cum)).astype(bf16)
+        mid_cum = 0.5 * last
+        q_scr[:, c] = (query[:, c].astype(f32) * jnp.exp(cum - mid_cum)).astype(bf16)
+        keys = (key * jnp.exp(mid_cum - cum)).astype(bf16)
         k_scr[:, c] = keys
-        st_send[c, :] = (dot(value[:, c], keys, TN) * jnp.exp(mid)).astype(bf16)
-        g = h // per
-        dec_send[g, h % per : h % per + 1, :] = last
-        if h == 0:
-            pl.semaphore_wait(barrier, n)
-        if h % per == per - 1:
-            for r in others:
-                decay_copy(g, r).start()
-                state_copy(g, r).start()
-            st_recv[g, 0] = st_send[owned(g, me), :]
-            dec_recv[g, 0] = dec_send[g]
-            if g == 0:
-                for copy in peer + local:
-                    copy.start()
+        st_send[c, :] = (dot(value[:, c], keys, TN) * jnp.exp(mid_cum)).astype(bf16)
+        dec_send[h // per, h % per : h % per + 1, :] = last
+
+    plane = n // 4
+    z, spot = me // plane, me % plane
+    upper = z // 2
+    first_near = 2 * upper * plane
+    is_mid = z == 1 + upper
+    far_mid, far_end = 2 - upper, 3 - 3 * upper
+    my_kind = jnp.where(is_mid, 0, 1)
+    near = 2 * plane
+    near_slots = near * cap
+
+    for move in moves[4:]:
+        move.wait()
+    top, count = routing.shape
+    owner = lax.broadcasted_iota(jnp.int32, (n, count), 0)
+    before = (
+        lax.broadcasted_iota(jnp.int32, (count, count), 0)
+        < lax.broadcasted_iota(jnp.int32, (count, count), 1)
+    ).astype(bf16)
+    used = jnp.zeros((n, 1), f32)
+    slot_rows, weight_rows = [], []
+    for k in range(top):
+        hot = (routing[k : k + 1, :] == owner).astype(f32)
+        rank = dot(hot.astype(bf16), before) + used
+        used = used + jnp.sum(hot, axis=1, keepdims=True)
+        slot_rows.append(
+            jnp.sum(hot * (rank + owner.astype(f32) * cap), axis=0, keepdims=True)
+        )
+        weight_rows.append(weight[k : k + 1, :])
+
+    def tables(index, slots, weights):
+        line = lax.broadcasted_iota(jnp.int32, (near_slots, count), 0).astype(f32)
+        chosen = jnp.zeros((near_slots, count), f32)
+        scale = jnp.zeros((near_slots, count), f32)
+        for slot, share in zip(slots, weights):
+            mine = slot == line
+            chosen = jnp.where(mine, 1.0, chosen)
+            scale = jnp.where(mine, share, scale)
+        high = scale.astype(bf16)
+        pick[index] = chosen.astype(bf16)
+        comb[index, 0] = high
+        comb[index, 1] = (scale - high.astype(f32)).astype(bf16)
+
+    def base_of(first):
+        return (first * cap).astype(f32)
+
+    tables(0, [slot - base_of(first_near) for slot in slot_rows], weight_rows)
+    info_send[...] = jnp.zeros_like(info_send)
+    for k in range(top):
+        info_send[k : k + 1, :count] = slot_rows[k] - base_of(near - first_near)
+        info_send[top + k : top + k + 1, :count] = weight_rows[k]
+
+    pl.semaphore_wait(barrier, n)
+    for g in range(groups):
+        for r in others:
+            decay_copy(g, r).start()
+            state_copy(g, r).start()
+    info_copy = pltpu.make_async_remote_copy(
+        src_ref=info_send, dst_ref=info_recv.at[my_kind],
+        send_sem=is_sem, recv_sem=ir_sem.at[my_kind],
+        device_id={"sp": far_mid * plane + spot}, device_id_type=MESH,
+    )
+    info_copy.start()
+    for copy in peer:
+        copy.start()
+    for g in range(groups):
+        st_recv[g, 0] = st_send[owned(g, me), :]
+        dec_recv[g, 0] = dec_send[g]
 
     for h in range(heads):
         c = slice(h * HEAD_DIM, (h + 1) * HEAD_DIM)
         scores = jnp.where(causal, dot(q_scr[:, c], k_scr[:, c], NT), 0.0).astype(bf16)
         ho[:, c] = dot(scores, value[:, c])
-
-    slots = n * cap
-    for move in moves[4:]:
-        move.wait()
-    top, count = routing.shape
-    eye = lax.broadcasted_iota(jnp.int32, (count, count), 0) == lax.broadcasted_iota(
-        jnp.int32, (count, count), 1
-    )
-
-    def column(line):
-        return jnp.sum(jnp.where(eye, line, 0.0), axis=1, keepdims=True)
-
-    expert = lax.broadcasted_iota(jnp.int32, (count, n), 1).astype(f32)
-    slot_of = lax.broadcasted_iota(jnp.int32, (count, slots), 1)
-    before = (
-        lax.broadcasted_iota(jnp.int32, (count, count), 0)
-        > lax.broadcasted_iota(jnp.int32, (count, count), 1)
-    ).astype(bf16)
-    used = jnp.zeros((1, n), f32)
-    picks = jnp.zeros((count, slots), f32)
-    combine = jnp.zeros((count, slots), f32)
-    for k in range(top):
-        hot = (column(routing[k : k + 1, :].astype(f32)) == expert).astype(f32)
-        rank = dot(before, hot.astype(bf16)) + used
-        used = used + jnp.sum(hot, axis=0, keepdims=True)
-        slot = jnp.sum(hot * (rank + expert * cap), axis=1, keepdims=True)
-        mine = slot.astype(jnp.int32) == slot_of
-        picks = jnp.where(mine, 1.0, picks)
-        combine = jnp.where(mine, column(weight[k : k + 1, :]), combine)
-    high = combine.astype(bf16)
-    both = jnp.concatenate([high, (combine - high.astype(f32)).astype(bf16)], axis=0)
-
+        g = gate[:, c].astype(f32)
+        gated[:, c] = gain[:, c] * (g / (1.0 + jnp.exp(-g)))
+
+    @pl.when(is_mid)
+    def _():
+        for kind in range(2):
+            pltpu.make_async_remote_copy(
+                src_ref=info_send, dst_ref=info_recv.at[kind],
+                send_sem=is_sem, recv_sem=ir_sem.at[kind],
+                device_id={"sp": far_mid * plane + spot}, device_id_type=MESH,
+            ).wait_recv()
+            tables(
+                1 + kind,
+                [info_recv[kind, k : k + 1, :count] for k in range(top)],
+                [info_recv[kind, top + k : top + k + 1, :count] for k in range(top)],
+            )
+
+    own_head = me * piece // HEAD_DIM
     for g in range(groups):
         for r in others:
             decay_copy(g, r).wait_recv()
             state_copy(g, r).wait_recv()
-        own_head = me * piece // HEAD_DIM
 
         def prefix(p, acc):
             r = 0
@@ -208,7 +253,7 @@
             ret_send[g, p] = (acc * jnp.exp(0.5 * last)).astype(bf16)
             return acc * jnp.exp(last) + st_recv[g, r].astype(f32)
 
-        lax.fori_loop(0, n, prefix, jnp.zeros((piece, HEAD_DIM), f32))
+        lax.fori_loop(0, n, prefix, jnp.zeros((piece, HEAD_DIM), f32), unroll=n <= 16)
         for r in others:
             back_copy(g, r).start()
         ret_recv[owned(g, me), :] = ret_send[g, me]
@@ -220,8 +265,7 @@
                 back_from(h // per, r).wait_recv()
         out = ho[:, c] + dot(q_scr[:, c], ret_recv[c, :], NT)
         out = out * lax.rsqrt(jnp.mean(out * out, axis=1, keepdims=True) + epsilon)
-        g = gate[:, c].astype(f32)
-        out = (out * gain[:, c] * (g / (1.0 + jnp.exp(-g)))).astype(bf16)
+        out = (out * gated[:, c]).astype(bf16)
         mixed[0, :, c] = out[:half]
         mixed[1, :, c] = out[half:]
 
@@ -248,57 +292,127 @@
     updated = (residual[...].astype(f32) + proj[...]).astype(bf16)
     updated = updated.astype(f32)
     proj[...] = updated
-    normed = (
+    normed[...] = (
         updated
         * lax.rsqrt(jnp.mean(updated * updated, axis=1, keepdims=True) + epsilon)
         * ffn_gain[...]
     ).astype(bf16)
-    outbox[...] = dot(picks.astype(bf16), normed, TN).astype(bf16)
-
-    sets = [
-        [r for r in range(n - 1, -1, -1) if (r ^ (r >> 1)) & 1 == which] for which in range(2)
-    ]
-    place = {r: i for i, r in enumerate(sets[0] + sets[1])}
+
+    chunks = 2
+    wide = total // chunks
+
+    def part_of(k):
+        return pl.ds(k * wide, wide)
+
+    def dense_copy(kind, k, relay):
+        return pltpu.make_async_remote_copy(
+            src_ref=normed.at[:, part_of(k)], dst_ref=dense_in.at[kind, :, part_of(k)],
+            send_sem=vs_sem.at[k], recv_sem=vr_sem.at[kind, k],
+            device_id={"sp": relay * plane + spot}, device_id_type=MESH,
+        )
 
     def block(r):
-        return pl.ds(place[r] * cap, cap)
+        return pl.ds(r * cap, cap)
+
+    def local_rows(device):
+        return rows_of(device - first_near, cap)
 
     def send_copy(r):
         return pltpu.make_async_remote_copy(
-            src_ref=outbox.at[rows_of(partner(me, r), cap)], dst_ref=arrived.at[block(r)],
+            src_ref=outbox.at[local_rows(partner(me, r))], dst_ref=arrived.at[block(r)],
             send_sem=xs_sem.at[r], recv_sem=xr_sem.at[r],
             device_id={"sp": partner(me, r)}, device_id_type=MESH,
         )
 
+    def relay_copy(kind, r, k):
+        return pltpu.make_async_remote_copy(
+            src_ref=relay_out.at[kind, local_rows(partner(me, r)), part_of(k)],
+            dst_ref=arrived.at[block(near + kind * plane + r % plane), part_of(k)],
+            send_sem=fs_sem.at[kind, r, k], recv_sem=fr_sem.at[kind, r % plane, k],
+            device_id={"sp": partner(me, r)}, device_id_type=MESH,
+        )
+
+    def relay_from(kind, r, k):
+        return pltpu.make_async_remote_copy(
+            src_ref=relay_out.at[kind, local_rows(partner(me, r)), part_of(k)],
+            dst_ref=arrived.at[block(near + kind * plane + r), part_of(k)],
+            send_sem=fs_sem.at[kind, r, k], recv_sem=fr_sem.at[kind, r, k],
+            device_id={"sp": (1 + upper) * plane + partner(spot, r)}, device_id_type=MESH,
+        )
+
     def answer_copy(r):
         return pltpu.make_async_remote_copy(
-            src_ref=result.at[block(r)], dst_ref=returned.at[rows_of(me, cap)],
+            src_ref=result.at[block(r)], dst_ref=returned.at[local_rows(me)],
             send_sem=ys_sem.at[r], recv_sem=yr_sem.at[r],
             device_id={"sp": partner(me, r)}, device_id_type=MESH,
         )
 
     def answer_from(r):
         return pltpu.make_async_remote_copy(
-            src_ref=result.at[block(r)], dst_ref=returned.at[rows_of(partner(me, r), cap)],
+            src_ref=result.at[block(r)], dst_ref=returned.at[local_rows(partner(me, r))],
             send_sem=ys_sem.at[r], recv_sem=yr_sem.at[r],
             device_id={"sp": partner(me, r)}, device_id_type=MESH,
         )
 
-    for r in sets[0] + sets[1]:
-        if r:
-            send_copy(r).start()
-    arrived[block(0), :] = outbox[rows_of(me, cap), :]
-    for copy in peer + local:
-        copy.wait()
+    def gather_copy(kind, r, k):
+        return pltpu.make_async_remote_copy(
+            src_ref=result.at[block(near + kind * plane + r), part_of(k)],
+            dst_ref=relay_in.at[kind, local_rows(me), part_of(k)],
+            send_sem=gs_sem.at[kind, r, k], recv_sem=gr_sem.at[kind, my_kind * plane + r, k],
+            device_id={"sp": (1 + upper) * plane + partner(spot, r)}, device_id_type=MESH,
+        )
+
+    def gather_from(kind, r, k):
+        return pltpu.make_async_remote_copy(
+            src_ref=result.at[block(near + kind * plane + r % plane), part_of(k)],
+            dst_ref=relay_in.at[kind, local_rows(partner(me, r)), part_of(k)],
+            send_sem=gs_sem.at[kind, r % plane, k], recv_sem=gr_sem.at[kind, r, k],
+            device_id={"sp": partner(me, r)}, device_id_type=MESH,
+        )
+
+    def home_copy(kind, k):
+        return pltpu.make_async_remote_copy(
+            src_ref=dense_out.at[kind, :, part_of(k)], dst_ref=dense_ret.at[:, part_of(k)],
+            send_sem=es_sem.at[kind, k], recv_sem=er_sem.at[k],
+            device_id={"sp": (far_mid, far_end)[kind] * plane + spot}, device_id_type=MESH,
+        )
+
+    @pl.when(is_mid)
+    def _():
+        for k in range(chunks):
+            dense_copy(0, k, far_mid).start()
+
+    outbox[...] = dot(pick[0], normed[...]).astype(bf16)
+    for r in range(near - 1, plane - 1, -1):
+        send_copy(r).start()
+
+    @pl.when(jnp.logical_not(is_mid))
+    def _():
+        for k in range(chunks):
+            dense_copy(1, k, far_mid).start()
+
+    for r in range(plane - 1, 0, -1):
+        send_copy(r).start()
+    arrived[block(0), :] = outbox[local_rows(me), :]
+
+    def relay(kind):
+        @pl.when(is_mid)
+        def _():
+            for k in range(chunks):
+                dense_copy(kind, k, far_mid).wait_recv()
+                relay_out[kind, :, part_of(k)] = dot(
+                    pick[1 + kind], dense_in[kind, :, part_of(k)]
+                ).astype(bf16)
+                for r in range(near - 1, 0, -1):
+                    relay_copy(kind, r, k).start()
+                arrived[block(near + kind * plane), part_of(k)] = relay_out[
+                    kind, local_rows(me), part_of(k)
+                ]
+
     inner = wg.shape[2]
     narrow = 256
-    first = 0
-    for group in sets:
-        for r in group:
-            if r:
-                send_copy(r).wait_recv()
-        part = slice(first, first + len(group) * cap)
-        first = first + len(group) * cap
+
+    def raise_up(part):
         for s in range(2):
 
             @pl.loop(0, inner // narrow)
@@ -308,27 +422,83 @@
                 u = dot(arrived[part, :], wu[s, :, cols])
                 hidden[s, part, cols] = (g / (1.0 + jnp.exp(-g)) * u).astype(bf16)
 
-        @pl.loop(0, total // tile)
+    def bring_down(part, k):
+        @pl.loop(0, wide // tile)
         def _(j):
-            cols = rows_of(j, tile)
+            cols = pl.ds(pl.multiple_of(k * wide + j * tile, tile), tile)
             result[part, cols] = (
                 dot(hidden[0, part, :], wd[0, :, cols]) + dot(hidden[1, part, :], wd[1, :, cols])
             ).astype(bf16)
 
-        for r in group:
-            if r:
-                answer_copy(r).start()
-
-    returned[rows_of(me, cap), :] = result[block(0), :]
-    for r in sets[0] + sets[1]:
-        if r:
-            answer_from(r).wait_recv()
+    def far_group(kind):
+        for r in range(plane):
+            for k in range(chunks):
+                if r:
+                    relay_from(kind, r, k).wait_recv()
+                else:
+
+                    @pl.when(jnp.logical_not(is_mid))
+                    def _():
+                        relay_from(kind, r, k).wait_recv()
+
+        part = slice((near + kind * plane) * cap, (near + (kind + 1) * plane) * cap)
+        raise_up(part)
+        for k in range(chunks):
+            bring_down(part, k)
+            for r in range(plane - 1, 0, -1):
+                gather_copy(kind, r, k).start()
+
+            @pl.when(jnp.logical_not(is_mid))
+            def _():
+                gather_copy(kind, 0, k).start()
+
+            @pl.when(is_mid)
+            def _():
+                relay_in[kind, local_rows(me), part_of(k)] = result[
+                    block(near + kind * plane), part_of(k)
+                ]
+
+    relay(0)
+    for copy in peer + local:
+        copy.wait()
+    for r in range(1, near):
+        send_copy(r).wait_recv()
+    raise_up(slice(0, near_slots))
+    for k in range(chunks):
+        bring_down(slice(0, near_slots), k)
+    for r in range(near - 1, 0, -1):
+        answer_copy(r).start()
+    returned[local_rows(me), :] = result[block(0), :]
+    relay(1)
+    far_group(0)
+    far_group(1)
+
+    @pl.when(is_mid)
+    def _():
+        for kind in range(2):
+            for k in range(chunks):
+                for r in range(1, near):
+                    gather_from(kind, r, k).wait_recv()
+                rows = relay_in[kind, :, part_of(k)]
+                dense_out[kind, :, part_of(k)] = (
+                    dot(comb[1 + kind, 0], rows, TN) + dot(comb[1 + kind, 1], rows, TN)
+                ).astype(bf16)
+                home_copy(kind, k).start()
+
+    for r in range(1, near):
+        answer_from(r).wait_recv()
 
     @pl.loop(0, total // tile)
     def _(j):
         cols = rows_of(j, tile)
-        back = dot(both, returned[:, cols])
-        layer_out[:, cols] = (proj[:, cols] + (back[:count] + back[count:])).astype(bf16)
+        rows = returned[:, cols]
+        proj[:, cols] = proj[:, cols] + (dot(comb[0, 0], rows, TN) + dot(comb[0, 1], rows, TN))
+
+    for k in range(chunks):
+        home_copy(0, k).wait_recv()
+        layer_out[:, part_of(k)] = (
+            proj[:, part_of(k)] + dense_ret[:, part_of(k)].astype(f32)
+        ).astype(bf16)
 
     for g in range(groups):
         for r in others:
@@ -336,9 +506,26 @@
             state_copy(g, r).wait_send()
             back_copy(g, r).wait_send()
 
-    for r in range(1, n):
+    info_copy.wait_send()
+    for k in range(chunks):
+        dense_copy(0, k, far_mid).wait_send()
+    for r in range(1, near):
         send_copy(r).wait_send()
         answer_copy(r).wait_send()
+    for kind in range(2):
+        for k in range(chunks):
+            for r in range(1, plane):
+                gather_copy(kind, r, k).wait_send()
+
+            @pl.when(jnp.logical_not(is_mid))
+            def _():
+                gather_copy(kind, 0, k).wait_send()
+
+            @pl.when(is_mid)
+            def _():
+                for r in range(1, near):
+                    relay_copy(kind, r, k).wait_send()
+                home_copy(kind, k).wait_send()
 
 
 def solution(mesh):
@@ -356,7 +543,10 @@
         half, model = residual_in.shape
         cap = 2 * half * routing.shape[1] // n
         cap = -(-cap // 16) * 16
-        slots = n * cap
+        plane = n // 4
+        near = 2 * plane
+        slots, near_slots = n * cap, near * cap
+        chunks = 2
         groups = 2 if heads % 2 == 0 and width // n % 32 == 0 else 1
         piece = width // n // groups
         inner = expert_gate.shape[2]
@@ -393,16 +583,32 @@
                 pltpu.VMEM((2, model, inner), bf16),
                 pltpu.VMEM((2, model, inner), bf16),
                 pltpu.VMEM((2, inner, model), bf16),
-                pltpu.VMEM((slots, model), bf16),
+                pltpu.VMEM((length, width), f32),
+                pltpu.VMEM((half, model), bf16),
+                pltpu.VMEM((3, near_slots, half), bf16),
+                pltpu.VMEM((3, 2, near_slots, half), bf16),
+                pltpu.VMEM((-(-2 * top // 8) * 8, -(-half // 128) * 128), f32),
+                pltpu.VMEM((2, -(-2 * top // 8) * 8, -(-half // 128) * 128), f32),
+                pltpu.VMEM((near_slots, model), bf16),
                 pltpu.VMEM((slots, model), bf16),
                 pltpu.VMEM((2, slots, inner), bf16),
                 pltpu.VMEM((slots, model), bf16),
-                pltpu.VMEM((slots, model), bf16),
+                pltpu.VMEM((near_slots, model), bf16),
+                pltpu.VMEM((2, half, model), bf16),
+                pltpu.VMEM((2, near_slots, model), bf16),
+                pltpu.VMEM((2, near_slots, model), bf16),
+                pltpu.VMEM((2, half, model), bf16),
+                pltpu.VMEM((half, model), bf16),
                 dma((10,)), dma,
                 dma((groups, n)), dma((groups, n)), dma((groups, n)),
                 dma((groups, n)), dma((groups, n)), dma((groups, n)),
                 dma, dma, dma((3,)), dma((3,)), dma((3,)),
-                dma((n,)), dma((n,)), dma((n,)), dma((n,)),
+                dma, dma((2,)),
+                dma((near,)), dma((near,)), dma((near,)), dma((near,)),
+                dma((chunks,)), dma((2, chunks)),
+                dma((2, near, chunks)), dma((2, plane, chunks)),
+                dma((2, plane, chunks)), dma((2, near, chunks)),
+                dma((2, chunks)), dma((chunks,)),
             ],
             compiler_params=pltpu.CompilerParams(
                 collective_id=0, has_side_effects=True, vmem_limit_bytes=60 << 20

time: 79.5 us -> 72 us (0.906)
  Pallas kernels: 77.7 us -> 70.2 us
    pallas_call x1, Pallas kernels: 77.7 us -> 70.2 us  [body(): pl.pallas_call(functools.partial(layer_kernel, n, cap), out_shape=jax.Sha...]
where the time goes in v1:
time: 72 us; the launch traced here: 71.9 us
  Pallas kernels  70.2 us (98%)
  local copies, waits for them, and re-layouts  1.67 us (2%)
    pallas_call x1, Pallas kernels, body(): pl.pallas_call(functools.partial(layer_kernel, n, cap), out_shape=jax.Sha...  70.2 us
    unnamed x1, local copies, waits for them, and re-layouts  1.67 us

profile of v1, /device:TPU:0, one launch (start us, length us, event | category | flops | bytes accessed | tf_op | source)
XLA Modules:
  0.0 71.9 jit_solution(10850521386479428844)
XLA Ops:
  0.0 70.2 %shard_map.136 = bf16[64,2048]{1,0:T(8,128)(2,1)} custom-call(bf16[128,1024]{1,0:T(8,128)(2,1)} %query_h.1, bf16[128,1024]{1,0:T(8,128)(2,1)} %logit_h.1, bf16[128,1024]{1,0:T(8,128)(2,1)} %value_h.1, bf16[128,1024]{1,0:T(8,128)(2,1)} %gate_h.1, f32[1,1024]{1,0:T(1,128)} %bitcast.6, f32[1,1024]{1,0:T(1,128)} %bitcast.7, bf16[64,2048]{1,0:T(8,128)(2,1)} %residual_h.1, ...), custom_call_target="tpu_custom_call" | custom-call | tf_op jit(solution)/shard_map/pallas_call | solution.py:554
  70.2 1.7 %copy.16 = bf16[64,2048]{1,0:T(8,128)(2,1)} copy(bf16[64,2048]{1,0:T(8,128)(2,1)} %shard_map.136) | data formatting | bytes 524288

commit v2 on v1

v2 whole, which is shorter than its diff:
```python
import functools

import jax
import jax.numpy as jnp
from jax import lax
from jax.experimental import pallas as pl
from jax.experimental.pallas import tpu as pltpu
from jax.sharding import PartitionSpec as P

HEAD_DIM = 128
MESH = pl.DeviceIdType.MESH
epsilon = 1e-06
f32 = jnp.float32
bf16 = jnp.bfloat16
NT = (((1,), (1,)), ((), ()))
TN = (((0,), (0,)), ((), ()))


def dot(a, b, dims=(((1,), (0,)), ((), ())), precision=None):
    return lax.dot_general(a, b, dims, precision=precision, preferred_element_type=f32)


def rows_of(index, count):
    return pl.ds(pl.multiple_of(index * count, count), count)


def greet(n):
    me, core = lax.axis_index("sp"), lax.axis_index("tp")
    barrier = pltpu.get_barrier_semaphore()
    pl.semaphore_signal(barrier, inc=1, device_id={"tp": 1 - core}, device_id_type=MESH)

    @pl.loop(1, n)
    def _(r):
        pl.semaphore_signal(
            barrier, inc=1, device_id={"sp": lax.rem(me + r, n)}, device_id_type=MESH
        )

    return barrier


def partner(me, r):
    other = me
    step = 1
    while step <= r:
        if r & step:
            other = other + step * (1 - 2 * (me // step % 2))
        step *= 2
    return other


def arrivals(ref, sem):
    peer = {"tp": 1 - lax.axis_index("tp")}
    pltpu.make_async_remote_copy(ref, ref, sem, sem, device_id=peer, device_id_type=MESH).wait_recv()


def departures(ref, sem):
    peer = {"tp": 1 - lax.axis_index("tp")}
    pltpu.make_async_remote_copy(ref, ref, sem, sem, device_id=peer, device_id_type=MESH).wait_send()


def layer_kernel(
    n, cap,
    query_h, logit_h, value_h, gate_h, bound_h, gain_h, residual_h, ffn_gain_h, routing_h,
    weight_h, w_hbm, g_hbm, u_hbm, d_hbm,
    layer_out,
    query, logit, value, gate, bound, gain, residual, ffn_gain, routing, weight,
    w_out, q_scr, k_scr, ho, st_send, st_recv, dec_send, dec_recv, ret_send, ret_recv,
    mixed, regrouped, proj,
    wg, wu, wd, gated, normed, pick, comb, pick_far, comb_far, info_send, info_recv,
    outbox, arrived, acc, hidden, result, returned, dense_in, far_out, part_in, part_add, dense_out, dense_ret,
    in_sem, w_sem, s_sem, r_sem, ds_sem, dr_sem, bs_sem, br_sem, ms_sem, mr_sem,
    l_sem, ps_sem, pr_sem, is_sem, ir_sem, xs_sem, xr_sem, ys_sem, yr_sem,
    vs_sem, vr_sem, ws_sem, fs_sem, fr_sem, gs_sem, gr_sem, as_sem, ar_sem, es_sem, er_sem,
):
    me, core = lax.axis_index("sp"), lax.axis_index("tp")
    length, width = query.shape
    heads = width // HEAD_DIM
    groups, piece = st_recv.shape[0], st_recv.shape[2]
    per = heads // groups
    half = length // 2
    moves = [
        pltpu.make_async_copy(src, dst, in_sem.at[i])
        for i, (src, dst) in enumerate((
            (logit_h, logit), (bound_h, bound), (query_h, query), (value_h, value),
            (routing_h, routing), (weight_h, weight), (gate_h, gate), (gain_h, gain),
            (residual_h, residual), (ffn_gain_h, ffn_gain),
        ))
    ]
    for move in moves:
        move.start()
    barrier = greet(n)
    w_copy = pltpu.make_async_copy(w_hbm, w_out, w_sem)
    homes = ((g_hbm, wg), (u_hbm, wu), (d_hbm, wd))
    local = [
        pltpu.make_async_copy(src.at[0], dst.at[0], l_sem.at[i])
        for i, (src, dst) in enumerate(homes)
    ]
    peer = [
        pltpu.make_async_remote_copy(
            src_ref=src.at[0], dst_ref=dst.at[1],
            send_sem=ps_sem.at[i], recv_sem=pr_sem.at[i],
            device_id={"tp": 1 - core}, device_id_type=MESH,
        )
        for i, (src, dst) in enumerate(homes)
    ]
    w_copy.start()
    for copy in local:
        copy.start()
    for move in moves[:4]:
        move.wait()

    row = lax.broadcasted_iota(jnp.int32, (length, length), 0)
    col = lax.broadcasted_iota(jnp.int32, (length, length), 1)
    causal = row >= col
    tri = causal.astype(f32)
    def owned(g, index):
        return pl.ds(pl.multiple_of(g * per * HEAD_DIM + index * piece, piece), piece)

    def state_copy(g, r):
        return pltpu.make_async_remote_copy(
            src_ref=st_send.at[owned(g, partner(me, r))], dst_ref=st_recv.at[g, r],
            send_sem=s_sem, recv_sem=r_sem.at[g],
            device_id={"sp": partner(me, r)}, device_id_type=MESH,
        )

    def decay_copy(g, r):
        return pltpu.make_async_remote_copy(
            src_ref=dec_send.at[g], dst_ref=dec_recv.at[g, r],
            send_sem=ds_sem, recv_sem=dr_sem.at[g],
            device_id={"sp": partner(me, r)}, device_id_type=MESH,
        )

    def back_copy(g, r):
        return pltpu.make_async_remote_copy(
            src_ref=ret_send.at[g, partner(me, r)], dst_ref=ret_recv.at[owned(g, me)],
            send_sem=bs_sem, recv_sem=br_sem.at[g],
            device_id={"sp": partner(me, r)}, device_id_type=MESH,
        )

    others = range(n - 1, 0, -1)

    for h in range(heads):
        c = slice(h * HEAD_DIM, (h + 1) * HEAD_DIM)
        key = (1.0 - bound[:, c]) / (1.0 + jnp.exp(logit[:, c].astype(f32)))
        cum = dot(tri, jnp.log1p(-key), precision=lax.Precision.HIGHEST)
        last = cum[length - 1 :, :]
        mid_cum = 0.5 * last
        q_scr[:, c] = (query[:, c].astype(f32) * jnp.exp(cum - mid_cum)).astype(bf16)
        keys = (key * jnp.exp(mid_cum - cum)).astype(bf16)
        k_scr[:, c] = keys
        st_send[c, :] = (dot(value[:, c], keys, TN) * jnp.exp(mid_cum)).astype(bf16)
        dec_send[h // per, h % per : h % per + 1, :] = last

    plane = n // 4
    z, spot = me // plane, me % plane
    upper = z // 2
    first_near = 2 * upper * plane
    is_mid = z == 1 + upper
    far_mid, far_end = 2 - upper, 3 - 3 * upper
    my_kind = jnp.where(is_mid, 0, 1)
    near = 2 * plane
    near_slots = near * cap

    for move in moves[4:]:
        move.wait()
    top, count = routing.shape
    owner = lax.broadcasted_iota(jnp.int32, (n, count), 0)
    before = (
        lax.broadcasted_iota(jnp.int32, (count, count), 0)
        < lax.broadcasted_iota(jnp.int32, (count, count), 1)
    ).astype(bf16)
    used = jnp.zeros((n, 1), f32)
    slot_rows, weight_rows = [], []
    for k in range(top):
        hot = (routing[k : k + 1, :] == owner).astype(f32)
        rank = dot(hot.astype(bf16), before) + used
        used = used + jnp.sum(hot, axis=1, keepdims=True)
        slot_rows.append(
            jnp.sum(hot * (rank + owner.astype(f32) * cap), axis=0, keepdims=True)
        )
        weight_rows.append(weight[k : k + 1, :])

    eye = lax.broadcasted_iota(jnp.int32, (count, count), 0) == lax.broadcasted_iota(
        jnp.int32, (count, count), 1
    )

    def column(line):
        return jnp.sum(jnp.where(eye, line, 0.0), axis=1, keepdims=True)

    def tables(chosen_ref, scale_ref, slots, weights):
        lines = chosen_ref.shape[0]
        down = lax.broadcasted_iota(jnp.int32, (lines, count), 0).astype(f32)
        across = lax.broadcasted_iota(jnp.int32, (count, lines), 1).astype(f32)
        chosen = jnp.zeros((lines, count), f32)
        scale = jnp.zeros((count, lines), f32)
        for slot, share in zip(slots, weights):
            chosen = jnp.where(slot == down, 1.0, chosen)
            scale = jnp.where(column(slot) == across, column(share), scale)
        high = scale.astype(bf16)
        chosen_ref[...] = chosen.astype(bf16)
        scale_ref[:count, :] = high
        scale_ref[count:, :] = (scale - high.astype(f32)).astype(bf16)

    def combined(scale, rows):
        both = dot(scale, rows)
        return both[:count] + both[count:]

    def base_of(first):
        return (first * cap).astype(f32)

    tables(pick, comb, [slot - base_of(first_near) for slot in slot_rows], weight_rows)
    info_send[...] = jnp.zeros_like(info_send)
    for k in range(top):
        info_send[k : k + 1, :count] = slot_rows[k]
        info_send[top + k : top + k + 1, :count] = weight_rows[k]

    pl.semaphore_wait(barrier, n)
    for g in range(groups):
        for r in others:
            decay_copy(g, r).start()
            state_copy(g, r).start()
    info_copies = [
        pltpu.make_async_remote_copy(
            src_ref=info_send, dst_ref=info_recv.at[my_kind],
            send_sem=is_sem, recv_sem=ir_sem.at[my_kind],
            device_id={"sp": to * plane + spot}, device_id_type=MESH,
        )
        for i, to in enumerate((far_mid, far_end))
    ]
    for copy in info_copies:
        copy.start()
    for copy in peer:
        copy.start()
    for g in range(groups):
        st_recv[g, 0] = st_send[owned(g, me), :]
        dec_recv[g, 0] = dec_send[g]

    for h in range(heads):
        c = slice(h * HEAD_DIM, (h + 1) * HEAD_DIM)
        scores = jnp.where(causal, dot(q_scr[:, c], k_scr[:, c], NT), 0.0).astype(bf16)
        ho[:, c] = dot(scores, value[:, c])
        g = gate[:, c].astype(f32)
        gated[:, c] = gain[:, c] * (g / (1.0 + jnp.exp(-g)))

    for kind in range(2):
        pltpu.make_async_remote_copy(
            src_ref=info_send, dst_ref=info_recv.at[kind],
            send_sem=is_sem, recv_sem=ir_sem.at[kind],
            device_id={"sp": far_mid * plane + spot}, device_id_type=MESH,
        ).wait_recv()
        tables(
            pick_far.at[kind],
            comb_far.at[kind],
            [info_recv[kind, k : k + 1, :count] - base_of(z * plane) for k in range(top)],
            [info_recv[kind, top + k : top + k + 1, :count] for k in range(top)],
        )

    own_head = me * piece // HEAD_DIM
    for g in range(groups):
        arrivals(dec_recv.at[g, pl.ds(1, n - 1)], dr_sem.at[g])
        arrivals(st_recv.at[g, pl.ds(1, n - 1)], r_sem.at[g])

        def prefix(p, acc):
            r = 0
            step = 1
            while step < n:
                r = r + step * ((me // step + p // step) % 2)
                step *= 2
            last = dec_recv[g, r, pl.ds(own_head, 1), :]
            ret_send[g, p] = (acc * jnp.exp(0.5 * last)).astype(bf16)
            return acc * jnp.exp(last) + st_recv[g, r].astype(f32)

        lax.fori_loop(0, n, prefix, jnp.zeros((piece, HEAD_DIM), f32), unroll=n <= 16)
        for r in others:
            back_copy(g, r).start()
        ret_recv[owned(g, me), :] = ret_send[g, me]

    total = w_out.shape[1]
    tile = 512
    band = per * HEAD_DIM

    def swap_copy(g):
        return pltpu.make_async_remote_copy(
            src_ref=mixed.at[1 - core, :, pl.ds(g * band, band)],
            dst_ref=regrouped.at[:, pl.ds(g * band, band)],
            send_sem=ms_sem, recv_sem=mr_sem.at[g],
            device_id={"tp": 1 - core}, device_id_type=MESH,
        )

    def project(which, source, g, first=False):
        depth = pl.ds(pl.multiple_of(which * width + g * band, band), band)
        for j in range(total // tile):
            cols = slice(j * tile, (j + 1) * tile)
            part = dot(source, w_out[depth, cols])
            proj[:, cols] = part if first else proj[:, cols] + part

    for g in range(groups):
        arrivals(ret_recv.at[pl.ds(g * band, (n - 1) * piece)], br_sem.at[g])
        for h in range(g * per, (g + 1) * per):
            c = slice(h * HEAD_DIM, (h + 1) * HEAD_DIM)
            out = ho[:, c] + dot(q_scr[:, c], ret_recv[c, :], NT)
            out = out * lax.rsqrt(jnp.mean(out * out, axis=1, keepdims=True) + epsilon)
            out = (out * gated[:, c]).astype(bf16)
            mixed[0, :, c] = out[:half]
            mixed[1, :, c] = out[half:]
        swap_copy(g).start()
        if g == 0:
            w_copy.wait()
        project(core, mixed[core, :, g * band : (g + 1) * band], g, first=g == 0)
        if g:
            swap_copy(g - 1).wait_recv()
            project(1 - core, regrouped[:, (g - 1) * band : g * band], g - 1)
    swap_copy(groups - 1).wait_recv()
    project(1 - core, regrouped[:, (groups - 1) * band :], groups - 1)
    updated = (residual[...].astype(f32) + proj[...]).astype(bf16)
    updated = updated.astype(f32)
    proj[...] = updated
    normed[...] = (
        updated
        * lax.rsqrt(jnp.mean(updated * updated, axis=1, keepdims=True) + epsilon)
        * ffn_gain[...]
    ).astype(bf16)

    chunks = vr_sem.shape[1]
    wide = total // chunks

    def part_of(k):
        return pl.ds(k * wide, wide)

    def dense_copy(kind, k, relay):
        return pltpu.make_async_remote_copy(
            src_ref=normed.at[:, part_of(k)], dst_ref=dense_in.at[kind, :, part_of(k)],
            send_sem=vs_sem, recv_sem=vr_sem.at[kind, k],
            device_id={"sp": relay * plane + spot}, device_id_type=MESH,
        )

    def block(r):
        return pl.ds(r * cap, cap)

    def local_rows(device):
        return rows_of(device - first_near, cap)

    def send_copy(r):
        return pltpu.make_async_remote_copy(
            src_ref=outbox.at[local_rows(partner(me, r))], dst_ref=arrived.at[block(r)],
            send_sem=xs_sem, recv_sem=xr_sem.at[r // plane],
            device_id={"sp": partner(me, r)}, device_id_type=MESH,
        )

    def forward_copy(kind, k):
        return pltpu.make_async_remote_copy(
            src_ref=dense_in.at[kind, :, part_of(k)], dst_ref=dense_in.at[kind, :, part_of(k)],
            send_sem=ws_sem, recv_sem=vr_sem.at[kind, k],
            device_id={"sp": partner(me, plane)}, device_id_type=MESH,
        )

    def scatter_copy(kind, r, k):
        return pltpu.make_async_remote_copy(
            src_ref=far_out.at[kind, rows_of(partner(spot, r), cap), part_of(k)],
            dst_ref=arrived.at[block(near + kind * plane + r), part_of(k)],
            send_sem=fs_sem, recv_sem=fr_sem.at[kind, k],
            device_id={"sp": partner(me, r)}, device_id_type=MESH,
        )

    def answer_copy(r, k):
        return pltpu.make_async_remote_copy(
            src_ref=result.at[block(r), part_of(k)],
            dst_ref=returned.at[local_rows(me), part_of(k)],
            send_sem=ys_sem, recv_sem=yr_sem.at[k],
            device_id={"sp": partner(me, r)}, device_id_type=MESH,
        )

    def gather_copy(kind, r, k):
        return pltpu.make_async_remote_copy(
            src_ref=result.at[block(near + kind * plane + r), part_of(k)],
            dst_ref=part_in.at[kind, rows_of(spot, cap), part_of(k)],
            send_sem=gs_sem, recv_sem=gr_sem.at[kind, k],
            device_id={"sp": partner(me, r)}, device_id_type=MESH,
        )

    def inward_copy(kind, k):
        return pltpu.make_async_remote_copy(
            src_ref=dense_out.at[kind, :, part_of(k)], dst_ref=part_add.at[kind, :, part_of(k)],
            send_sem=as_sem, recv_sem=ar_sem.at[kind, k],
            device_id={"sp": partner(me, plane)}, device_id_type=MESH,
        )

    def home_copy(kind, k):
        return pltpu.make_async_remote_copy(
            src_ref=dense_out.at[kind, :, part_of(k)], dst_ref=dense_ret.at[:, part_of(k)],
            send_sem=es_sem, recv_sem=er_sem.at[k],
            device_id={"sp": (far_mid, far_end)[kind] * plane + spot}, device_id_type=MESH,
        )

    not_mid = jnp.logical_not(is_mid)

    @pl.when(not_mid)
    def _():
        for k in range(chunks):
            dense_copy(1, k, far_mid).start()

    outbox[...] = dot(pick[...], normed[...]).astype(bf16)
    for r in range(plane - 1, 0, -1):
        send_copy(r).start()

    for r in range(near - 1, plane - 1, -1):
        send_copy(r).start()

    arrived[block(0), :] = outbox[local_rows(me), :]

    def forward(kind, k):
        @pl.when(is_mid)
        def _():
            dense_copy(kind, k, far_mid).wait_recv()
            forward_copy(kind, k).start()

    def scatter(kind, k):
        @pl.when(not_mid)
        def _():
            dense_copy(kind, k, far_mid).wait_recv()

        far_out[kind, :, part_of(k)] = dot(
            pick_far[kind], dense_in[kind, :, part_of(k)]
        ).astype(bf16)
        for r in range(plane - 1, 0, -1):
            scatter_copy(kind, r, k).start()
        arrived[block(near + kind * plane), part_of(k)] = far_out[
            kind, rows_of(spot, cap), part_of(k)
        ]

    inner = wg.shape[2]
    rows_each = plane * cap

    def rows_in(group):
        return slice(group * rows_each, (group + 1) * rows_each)

    def raise_up(group, k):
        part = rows_in(group)
        x = arrived[part, part_of(k)]
        for s in range(2):
            g = dot(x, wg[s, part_of(k), :])
            u = dot(x, wu[s, part_of(k), :])
            if k:
                g = g + acc[0, s]
                u = u + acc[1, s]
            if k < chunks - 1:
                acc[0, s] = g
                acc[1, s] = u
            else:
                hidden[s, part, :] = (g / (1.0 + jnp.exp(-g)) * u).astype(bf16)

    def bring_down(group, k):
        part = rows_in(group)
        result[part, part_of(k)] = (
            dot(hidden[0, part, :], wd[0, :, part_of(k)])
            + dot(hidden[1, part, :], wd[1, :, part_of(k)])
        ).astype(bf16)

    def near_answer(group, parts=range(4)):
        for k in parts:
            bring_down(group, k)
            for r in range((group + 1) * plane - 1, max(group * plane, 1) - 1, -1):
                answer_copy(r, k).start()
        if group == 0:
            returned[local_rows(me), :] = result[block(0), :]

    def far_arrive(kind, k):
        arrivals(
            arrived.at[pl.ds((near + kind * plane + 1) * cap, (plane - 1) * cap), part_of(k)],
            fr_sem.at[kind, k],
        )
        raise_up(2 + kind, k)

    def far_answer(kind, k):
        bring_down(2 + kind, k)
        for r in range(plane - 1, 0, -1):
            gather_copy(kind, r, k).start()
        part_in[kind, rows_of(spot, cap), part_of(k)] = result[
            block(near + kind * plane), part_of(k)
        ]

    def far_partial(kind, k):
        arrivals(
            part_in.at[kind, pl.ds(0, (plane - 1) * cap), part_of(k)], gr_sem.at[kind, k]
        )
        return combined(comb_far[kind], part_in[kind, :, part_of(k)])

    def inward(kind, k):
        @pl.when(not_mid)
        def _():
            dense_out[kind, :, part_of(k)] = far_partial(kind, k).astype(bf16)
            inward_copy(kind, k).start()

    def homeward(kind, k):
        @pl.when(is_mid)
        def _():
            mine = far_partial(kind, k)
            inward_copy(kind, k).wait_recv()
            dense_out[kind, :, part_of(k)] = (
                mine + part_add[kind, :, part_of(k)].astype(f32)
            ).astype(bf16)
            home_copy(kind, k).start()

    def start_mid():
        @pl.when(is_mid)
        def _():
            for k in range(chunks):
                dense_copy(0, k, far_mid).start()

    forward(1, 0)
    forward(1, 1)
    start_mid()
    for copy in peer + local:
        copy.wait()
    arrivals(arrived.at[pl.ds(cap, (plane - 1) * cap)], xr_sem.at[0])

    def near_raise(first):
        if first == 0:
            arrivals(arrived.at[pl.ds(plane * cap, plane * cap)], xr_sem.at[1])
        raise_up(1, first)
        raise_up(1, first + 1)

    def at_ends(step, value):
        @pl.when(not_mid)
        def _():
            step(value)

    def near_reply(first):
        near_answer(1, (first, first + 1))

    raise_up(0, 0)
    raise_up(0, 1)
    forward(1, 2)
    raise_up(0, 2)
    raise_up(0, 3)
    forward(1, 3)
    near_answer(0)
    at_ends(near_raise, 0)
    scatter(1, 0)
    at_ends(near_raise, 2)
    scatter(1, 1)
    at_ends(near_reply, 0)
    forward(0, 0)
    scatter(1, 2)
    at_ends(near_reply, 2)
    forward(0, 1)
    scatter(1, 3)
    far_arrive(1, 0)
    forward(0, 2)
    far_arrive(1, 1)
    forward(0, 3)
    far_arrive(1, 2)
    scatter(0, 0)
    far_arrive(1, 3)
    far_answer(1, 0)
    far_answer(1, 1)
    scatter(0, 1)
    far_answer(1, 2)
    far_answer(1, 3)

    @pl.when(is_mid)
    def _():
        near_raise(0)
        near_raise(2)

    scatter(0, 2)
    inward(1, 0)
    inward(1, 1)
    scatter(0, 3)
    inward(1, 2)
    inward(1, 3)

    @pl.when(is_mid)
    def _():
        near_reply(0)
        near_reply(2)

    far_arrive(0, 0)
    far_arrive(0, 1)
    far_arrive(0, 2)
    far_arrive(0, 3)
    far_answer(0, 0)
    far_answer(0, 1)
    far_answer(0, 2)
    far_answer(0, 3)
    homeward(1, 0)
    homeward(1, 1)
    homeward(1, 2)
    homeward(1, 3)
    inward(0, 0)
    inward(0, 1)
    inward(0, 2)
    inward(0, 3)
    homeward(0, 0)
    homeward(0, 1)
    homeward(0, 2)
    homeward(0, 3)
    for k in range(chunks):
        arrivals(returned.at[pl.ds(0, (near - 1) * cap), part_of(k)], yr_sem.at[k])
        home_copy(0, k).wait_recv()
        layer_out[:, part_of(k)] = (
            proj[:, part_of(k)]
            + combined(comb[...], returned[:, part_of(k)])
            + dense_ret[:, part_of(k)].astype(f32)
        ).astype(bf16)

    departures(dec_recv.at[:, pl.ds(1, n - 1)], ds_sem)
    departures(st_recv.at[:, pl.ds(1, n - 1)], s_sem)
    departures(ret_send.at[:, pl.ds(1, n - 1)], bs_sem)
    departures(info_recv, is_sem)
    departures(regrouped, ms_sem)
    departures(normed, vs_sem)
    departures(outbox.at[pl.ds(cap, (near - 1) * cap)], xs_sem)
    departures(result.at[pl.ds(cap, (near - 1) * cap)], ys_sem)
    departures(arrived.at[pl.ds(0, 2 * (plane - 1) * cap)], fs_sem)
    departures(result.at[pl.ds(0, 2 * (plane - 1) * cap)], gs_sem)

    @pl.when(not_mid)
    def _():
        departures(dense_out, as_sem)

    @pl.when(is_mid)
    def _():
        departures(dense_in, ws_sem)
        departures(dense_out, es_sem)


def solution(mesh):
    n = mesh.shape["sp"]
    vmem = pl.BlockSpec(memory_space=pltpu.VMEM)
    hbm = pl.BlockSpec(memory_space=pl.ANY)
    dma = pltpu.SemaphoreType.DMA

    def body(
        query, forget_logit, value, out_gate, lower_bound, head_gain, residual_in, w_out,
        ffn_gain, routing, route_weight, expert_gate, expert_up, expert_down,
    ):
        length, width = query.shape
        heads = width // HEAD_DIM
        half, model = residual_in.shape
        cap = 2 * half * routing.shape[1] // n
        cap = -(-cap // 16) * 16
        plane = n // 4
        near = 2 * plane
        slots, near_slots = n * cap, near * cap
        chunks = 4
        groups = max(
            g for g in (1, 2, 4) if heads % g == 0 and (g == 1 or width // n % (16 * g) == 0)
        )
        piece = width // n // groups
        inner = expert_gate.shape[2]
        top = routing.shape[1]
        return pl.pallas_call(
            functools.partial(layer_kernel, n, cap),
            out_shape=jax.ShapeDtypeStruct((half, model), bf16),
            in_specs=[hbm] * 14,
            out_specs=vmem,
            scratch_shapes=[
                pltpu.VMEM((length, width), bf16),
                pltpu.VMEM((length, width), bf16),
                pltpu.VMEM((length, width), bf16),
                pltpu.VMEM((length, width), bf16),
                pltpu.VMEM((1, width), f32),
                pltpu.VMEM((1, width), f32),
                pltpu.VMEM((half, model), bf16),
                pltpu.VMEM((1, model), f32),
                pltpu.VMEM((top, half), jnp.int32),
                pltpu.VMEM((top, half), f32),
                pltpu.VMEM(w_out.shape, bf16),
                pltpu.VMEM((length, width), bf16),
                pltpu.VMEM((length, width), bf16),
                pltpu.VMEM((length, width), f32),
                pltpu.VMEM((width, HEAD_DIM), bf16),
                pltpu.VMEM((groups, n, piece, HEAD_DIM), bf16),
                pltpu.VMEM((groups, heads // groups, HEAD_DIM), f32),
                pltpu.VMEM((groups, n, heads // groups, HEAD_DIM), f32),
                pltpu.VMEM((groups, n, piece, HEAD_DIM), bf16),
                pltpu.VMEM((width, HEAD_DIM), bf16),
                pltpu.VMEM((2, half, width), bf16),
                pltpu.VMEM((half, width), bf16),
                pltpu.VMEM((half, model), f32),
                pltpu.VMEM((2, model, inner), bf16),
                pltpu.VMEM((2, model, inner), bf16),
                pltpu.VMEM((2, inner, model), bf16),
                pltpu.VMEM((length, width), f32),
                pltpu.VMEM((half, model), bf16),
                pltpu.VMEM((near_slots, half), bf16),
                pltpu.VMEM((2 * half, near_slots), bf16),
                pltpu.VMEM((2, plane * cap, half), bf16),
                pltpu.VMEM((2, 2 * half, plane * cap), bf16),
                pltpu.VMEM((-(-2 * top // 8) * 8, -(-half // 128) * 128), f32),
                pltpu.VMEM((2, -(-2 * top // 8) * 8, -(-half // 128) * 128), f32),
                pltpu.VMEM((near_slots, model), bf16),
                pltpu.VMEM((slots, model), bf16),
                pltpu.VMEM((2, 2, plane * cap, inner), f32),
                pltpu.VMEM((2, slots, inner), bf16),
                pltpu.VMEM((slots, model), bf16),
                pltpu.VMEM((near_slots, model), bf16),
                pltpu.VMEM((2, half, model), bf16),
                pltpu.VMEM((2, plane * cap, model), bf16),
                pltpu.VMEM((2, plane * cap, model), bf16),
                pltpu.VMEM((2, half, model), bf16),
                pltpu.VMEM((2, half, model), bf16),
                pltpu.VMEM((half, model), bf16),
                dma((10,)), dma,
                dma, dma((groups,)), dma, dma((groups,)), dma, dma((groups,)),
                dma, dma((groups,)), dma((3,)), dma((3,)), dma((3,)),
                dma, dma((2,)), dma, dma((2,)), dma, dma((chunks,)),
                dma, dma((2, chunks)), dma, dma, dma((2, chunks)),
                dma, dma((2, chunks)), dma, dma((2, chunks)), dma, dma((chunks,)),
            ],
            compiler_params=pltpu.CompilerParams(
                collective_id=0, has_side_effects=True, vmem_limit_bytes=60 << 20
            ),
        )(
            query, forget_logit, value, out_gate, lower_bound[None], head_gain[None],
            residual_in, ffn_gain[None], routing.T, route_weight.T, w_out,
            expert_gate, expert_up, expert_down,
        )

    placed = (
        P("sp", "tp"), P("sp", "tp"), P("sp", "tp"), P("sp", "tp"), P("tp"), P("tp"),
        P(("sp", "tp"), None), P(), P(), P(("sp", "tp"), None), P(("sp", "tp"), None),
        P("sp", None, "tp"), P("sp", None, "tp"), P("sp", "tp", None),
    )
    return jax.shard_map(
        body, mesh=mesh, in_specs=placed, out_specs=P(("sp", "tp"), None), check_vma=False
    )
```

time: 72 us -> 69 us (0.958)
  Pallas kernels: 70.2 us -> 66.8 us
    pallas_call x1, Pallas kernels: 70.2 us -> 66.8 us  [body(): pl.pallas_call(functools.partial(layer_kernel, n, cap), out_shape=jax.Sha...]
where the time goes in v2:
time: 69 us; the launch traced here: 68.5 us
  Pallas kernels  66.8 us (97%)
  local copies, waits for them, and re-layouts  1.67 us (2%)
    pallas_call x1, Pallas kernels, body(): pl.pallas_call(functools.partial(layer_kernel, n, cap), out_shape=jax.Sha...  66.8 us
    unnamed x1, local copies, waits for them, and re-layouts  1.67 us

profile of v2, /device:TPU:0, one launch (start us, length us, event | category | flops | bytes accessed | tf_op | source)
XLA Modules:
  0.0 68.5 jit_solution(3306311923800911265)
XLA Ops:
  0.0 66.8 %shard_map.136 = bf16[64,2048]{1,0:T(8,128)(2,1)} custom-call(bf16[128,1024]{1,0:T(8,128)(2,1)} %query_h.1, bf16[128,1024]{1,0:T(8,128)(2,1)} %logit_h.1, bf16[128,1024]{1,0:T(8,128)(2,1)} %value_h.1, bf16[128,1024]{1,0:T(8,128)(2,1)} %gate_h.1, f32[1,1024]{1,0:T(1,128)} %bitcast.6, f32[1,1024]{1,0:T(1,128)} %bitcast.7, bf16[64,2048]{1,0:T(8,128)(2,1)} %residual_h.1, ...), custom_call_target="tpu_custom_call" | custom-call | tf_op jit(solution)/shard_map/pallas_call | solution.py:653
  66.8 1.7 %copy.16 = bf16[64,2048]{1,0:T(8,128)(2,1)} copy(bf16[64,2048]{1,0:T(8,128)(2,1)} %shard_map.136) | data formatting | bytes 524288

commit v3 on v2

--- a/solution.py
+++ b/solution.py
@@ -139,7 +139,7 @@
 
     others = range(n - 1, 0, -1)
 
-    for h in range(heads):
+    def local_state(h):
         c = slice(h * HEAD_DIM, (h + 1) * HEAD_DIM)
         key = (1.0 - bound[:, c]) / (1.0 + jnp.exp(logit[:, c].astype(f32)))
         cum = dot(tri, jnp.log1p(-key), precision=lax.Precision.HIGHEST)
@@ -150,6 +150,21 @@
         k_scr[:, c] = keys
         st_send[c, :] = (dot(value[:, c], keys, TN) * jnp.exp(mid_cum)).astype(bf16)
         dec_send[h // per, h % per : h % per + 1, :] = last
+
+    def send_states(first, last):
+        for g in range(first, last):
+            for r in others:
+                decay_copy(g, r).start()
+                state_copy(g, r).start()
+
+    early = (groups + 1) // 2
+    for h in range(early * per):
+        local_state(h)
+    pl.semaphore_wait(barrier, n)
+    send_states(0, early)
+    for h in range(early * per, heads):
+        local_state(h)
+    send_states(early, groups)
 
     plane = n // 4
     z, spot = me // plane, me % plane
@@ -214,11 +229,6 @@
         info_send[k : k + 1, :count] = slot_rows[k]
         info_send[top + k : top + k + 1, :count] = weight_rows[k]
 
-    pl.semaphore_wait(barrier, n)
-    for g in range(groups):
-        for r in others:
-            decay_copy(g, r).start()
-            state_copy(g, r).start()
     info_copies = [
         pltpu.make_async_remote_copy(
             src_ref=info_send, dst_ref=info_recv.at[my_kind],
@@ -399,6 +409,11 @@
         for k in range(chunks):
             dense_copy(1, k, far_mid).start()
 
+    @pl.when(is_mid)
+    def _():
+        for k in range(chunks // 2):
+            dense_copy(0, k, far_mid).start()
+
     outbox[...] = dot(pick[...], normed[...]).astype(bf16)
     for r in range(plane - 1, 0, -1):
         send_copy(r).start()
@@ -408,17 +423,20 @@
 
     arrived[block(0), :] = outbox[local_rows(me), :]
 
-    def forward(kind, k):
-        @pl.when(is_mid)
-        def _():
-            dense_copy(kind, k, far_mid).wait_recv()
-            forward_copy(kind, k).start()
-
     def scatter(kind, k):
-        @pl.when(not_mid)
-        def _():
-            dense_copy(kind, k, far_mid).wait_recv()
-
+        dense_copy(kind, k, far_mid).wait_recv()
+        far_out[kind, :, part_of(k)] = dot(
+            pick_far[kind], dense_in[kind, :, part_of(k)]
+        ).astype(bf16)
+        for r in range(plane - 1, 0, -1):
+            scatter_copy(kind, r, k).start()
+        arrived[block(near + kind * plane), part_of(k)] = far_out[
+            kind, rows_of(spot, cap), part_of(k)
+        ]
+
+    def relay(kind, k):
+        dense_copy(kind, k, far_mid).wait_recv()
+        forward_copy(kind, k).start()
         far_out[kind, :, part_of(k)] = dot(
             pick_far[kind], dense_in[kind, :, part_of(k)]
         ).astype(bf16)
@@ -456,12 +474,18 @@
             + dot(hidden[1, part, :], wd[1, :, part_of(k)])
         ).astype(bf16)
 
-    def near_answer(group, parts=range(4)):
-        for k in parts:
-            bring_down(group, k)
-            for r in range((group + 1) * plane - 1, max(group * plane, 1) - 1, -1):
-                answer_copy(r, k).start()
+    def near_arrive(group):
         if group == 0:
+            arrivals(arrived.at[pl.ds(cap, (plane - 1) * cap)], xr_sem.at[0])
+        else:
+            arrivals(arrived.at[pl.ds(plane * cap, plane * cap)], xr_sem.at[1])
+
+    def near_answer(group, parity):
+        for k in range(chunks):
+            for r in range(group * plane + parity, (group + 1) * plane, 2):
+                if r:
+                    answer_copy(r, k).start()
+        if group + parity == 0:
             returned[local_rows(me), :] = result[block(0), :]
 
     def far_arrive(kind, k):
@@ -486,115 +510,144 @@
         return combined(comb_far[kind], part_in[kind, :, part_of(k)])
 
     def inward(kind, k):
-        @pl.when(not_mid)
-        def _():
-            dense_out[kind, :, part_of(k)] = far_partial(kind, k).astype(bf16)
-            inward_copy(kind, k).start()
+        dense_out[kind, :, part_of(k)] = far_partial(kind, k).astype(bf16)
+        inward_copy(kind, k).start()
 
     def homeward(kind, k):
-        @pl.when(is_mid)
-        def _():
-            mine = far_partial(kind, k)
-            inward_copy(kind, k).wait_recv()
-            dense_out[kind, :, part_of(k)] = (
-                mine + part_add[kind, :, part_of(k)].astype(f32)
-            ).astype(bf16)
-            home_copy(kind, k).start()
-
-    def start_mid():
-        @pl.when(is_mid)
-        def _():
-            for k in range(chunks):
-                dense_copy(0, k, far_mid).start()
-
-    forward(1, 0)
-    forward(1, 1)
-    start_mid()
-    for copy in peer + local:
-        copy.wait()
-    arrivals(arrived.at[pl.ds(cap, (plane - 1) * cap)], xr_sem.at[0])
-
-    def near_raise(first):
-        if first == 0:
-            arrivals(arrived.at[pl.ds(plane * cap, plane * cap)], xr_sem.at[1])
-        raise_up(1, first)
-        raise_up(1, first + 1)
-
-    def at_ends(step, value):
-        @pl.when(not_mid)
-        def _():
-            step(value)
-
-    def near_reply(first):
-        near_answer(1, (first, first + 1))
-
-    raise_up(0, 0)
-    raise_up(0, 1)
-    forward(1, 2)
-    raise_up(0, 2)
-    raise_up(0, 3)
-    forward(1, 3)
-    near_answer(0)
-    at_ends(near_raise, 0)
-    scatter(1, 0)
-    at_ends(near_raise, 2)
-    scatter(1, 1)
-    at_ends(near_reply, 0)
-    forward(0, 0)
-    scatter(1, 2)
-    at_ends(near_reply, 2)
-    forward(0, 1)
-    scatter(1, 3)
-    far_arrive(1, 0)
-    forward(0, 2)
-    far_arrive(1, 1)
-    forward(0, 3)
-    far_arrive(1, 2)
-    scatter(0, 0)
-    far_arrive(1, 3)
-    far_answer(1, 0)
-    far_answer(1, 1)
-    scatter(0, 1)
-    far_answer(1, 2)
-    far_answer(1, 3)
+        mine = far_partial(kind, k)
+        inward_copy(kind, k).wait_recv()
+        dense_out[kind, :, part_of(k)] = (
+            mine + part_add[kind, :, part_of(k)].astype(f32)
+        ).astype(bf16)
+        home_copy(kind, k).start()
+
+    def mid_schedule():
+        relay(1, 0)
+        relay(1, 1)
+        for k in range(chunks // 2, chunks):
+            dense_copy(0, k, far_mid).start()
+        weights_arrive()
+        near_arrive(0)
+        raise_up(0, 0)
+        raise_up(0, 1)
+        relay(1, 2)
+        raise_up(0, 2)
+        raise_up(0, 3)
+        relay(1, 3)
+        bring_down(0, 0)
+        bring_down(0, 1)
+        relay(0, 0)
+        bring_down(0, 2)
+        bring_down(0, 3)
+        relay(0, 1)
+        far_arrive(1, 0)
+        far_arrive(1, 1)
+        relay(0, 2)
+        far_arrive(1, 2)
+        far_arrive(1, 3)
+        relay(0, 3)
+        far_answer(1, 0)
+        far_answer(1, 1)
+        far_answer(1, 2)
+        far_answer(1, 3)
+        near_arrive(1)
+        raise_up(1, 0)
+        raise_up(1, 1)
+        raise_up(1, 2)
+        raise_up(1, 3)
+        far_arrive(0, 0)
+        far_arrive(0, 1)
+        far_arrive(0, 2)
+        far_arrive(0, 3)
+        far_answer(0, 0)
+        far_answer(0, 1)
+        far_answer(0, 2)
+        far_answer(0, 3)
+        bring_down(1, 0)
+        bring_down(1, 1)
+        bring_down(1, 2)
+        bring_down(1, 3)
+        for group in range(2):
+            for parity in range(2):
+                near_answer(group, parity)
+        homeward(1, 0)
+        homeward(1, 1)
+        homeward(1, 2)
+        homeward(1, 3)
+        homeward(0, 0)
+        homeward(0, 1)
+        homeward(0, 2)
+        homeward(0, 3)
+
+    def end_schedule():
+        weights_arrive()
+        near_arrive(0)
+        raise_up(0, 0)
+        raise_up(0, 1)
+        raise_up(0, 2)
+        raise_up(0, 3)
+        scatter(1, 0)
+        bring_down(0, 0)
+        bring_down(0, 1)
+        scatter(1, 1)
+        bring_down(0, 2)
+        bring_down(0, 3)
+        near_arrive(1)
+        scatter(1, 2)
+        raise_up(1, 0)
+        raise_up(1, 1)
+        scatter(1, 3)
+        raise_up(1, 2)
+        raise_up(1, 3)
+        bring_down(1, 0)
+        bring_down(1, 1)
+        bring_down(1, 2)
+        bring_down(1, 3)
+        near_answer(0, 0)
+        near_answer(1, 0)
+        far_arrive(1, 0)
+        far_arrive(1, 1)
+        scatter(0, 0)
+        far_arrive(1, 2)
+        far_arrive(1, 3)
+        scatter(0, 1)
+        far_answer(1, 0)
+        far_answer(1, 1)
+        scatter(0, 2)
+        far_answer(1, 2)
+        far_answer(1, 3)
+        scatter(0, 3)
+        far_arrive(0, 0)
+        inward(1, 0)
+        far_arrive(0, 1)
+        inward(1, 1)
+        far_arrive(0, 2)
+        inward(1, 2)
+        far_arrive(0, 3)
+        inward(1, 3)
+        far_answer(0, 0)
+        far_answer(0, 1)
+        far_answer(0, 2)
+        far_answer(0, 3)
+        near_answer(1, 1)
+        near_answer(0, 1)
+        inward(0, 0)
+        inward(0, 1)
+        inward(0, 2)
+        inward(0, 3)
+
+    def weights_arrive():
+        for copy in peer + local:
+            copy.wait()
 
     @pl.when(is_mid)
     def _():
-        near_raise(0)
-        near_raise(2)
-
-    scatter(0, 2)
-    inward(1, 0)
-    inward(1, 1)
-    scatter(0, 3)
-    inward(1, 2)
-    inward(1, 3)
-
-    @pl.when(is_mid)
+        mid_schedule()
+
+    @pl.when(not_mid)
     def _():
-        near_reply(0)
-        near_reply(2)
-
-    far_arrive(0, 0)
-    far_arrive(0, 1)
-    far_arrive(0, 2)
-    far_arrive(0, 3)
-    far_answer(0, 0)
-    far_answer(0, 1)
-    far_answer(0, 2)
-    far_answer(0, 3)
-    homeward(1, 0)
-    homeward(1, 1)
-    homeward(1, 2)
-    homeward(1, 3)
-    inward(0, 0)
-    inward(0, 1)
-    inward(0, 2)
-    inward(0, 3)
-    homeward(0, 0)
-    homeward(0, 1)
-    homeward(0, 2)
-    homeward(0, 3)
+        end_schedule()
+
     for k in range(chunks):
         arrivals(returned.at[pl.ds(0, (near - 1) * cap), part_of(k)], yr_sem.at[k])
         home_copy(0, k).wait_recv()

time: 69 us -> 67.8 us (0.983)
  the two profiles are of different devices: /device:TPU:0 before, /device:TPU:10 now
where the time goes in v3:
time: 67.8 us; the launch traced here: 67.6 us
  Pallas kernels  66 us (97%)
  local copies, waits for them, and re-layouts  1.67 us (2%)
    pallas_call x1, Pallas kernels, body(): pl.pallas_call(functools.partial(layer_kernel, n, cap), out_shape=jax.Sha...  66 us
    unnamed x1, local copies, waits for them, and re-layouts  1.67 us

profile of v3, /device:TPU:10, one launch (start us, length us, event | category | flops | bytes accessed | tf_op | source)
XLA Modules:
  0.0 67.6 jit_solution(7630786234860164923)
XLA Ops:
  0.0 66.0 %shard_map.136 = bf16[64,2048]{1,0:T(8,128)(2,1)} custom-call(bf16[128,1024]{1,0:T(8,128)(2,1)} %query_h.1, bf16[128,1024]{1,0:T(8,128)(2,1)} %logit_h.1, bf16[128,1024]{1,0:T(8,128)(2,1)} %value_h.1, bf16[128,1024]{1,0:T(8,128)(2,1)} %gate_h.1, f32[1,1024]{1,0:T(1,128)} %bitcast.6, f32[1,1024]{1,0:T(1,128)} %bitcast.7, bf16[64,2048]{1,0:T(8,128)(2,1)} %residual_h.1, ...), custom_call_target="tpu_custom_call" | custom-call | tf_op jit(solution)/shard_map/pallas_call | solution.py:706
  66.0 1.7 %copy.16 = bf16[64,2048]{1,0:T(8,128)(2,1)} copy(bf16[64,2048]{1,0:T(8,128)(2,1)} %shard_map.136) | data formatting | bytes 524288

commit v4 on v3

--- a/solution.py
+++ b/solution.py
@@ -705,7 +705,7 @@
         top = routing.shape[1]
         return pl.pallas_call(
             functools.partial(layer_kernel, n, cap),
-            out_shape=jax.ShapeDtypeStruct((half, model), bf16),
+            out_shape=pltpu.VMEM((half, model), bf16),
             in_specs=[hbm] * 14,
             out_specs=vmem,
             scratch_shapes=[

time: 67.8 us -> 66.1 us (0.975)
  local copies, waits for them, and re-layouts: 1.67 us -> 0.71 us
  Pallas kernels: 66 us -> 65.3 us
    unnamed x1, local copies, waits for them, and re-layouts: 1.67 us -> 0.71 us
    pallas_call x1, Pallas kernels: 66 us -> 65.3 us  [body(): pl.pallas_call(functools.partial(layer_kernel, n, cap), out_shape=pltpu.V...]
where the time goes in v4:
time: 66.1 us; the launch traced here: 66 us
  Pallas kernels  65.3 us (99%)
  local copies, waits for them, and re-layouts  0.71 us (1%)
    pallas_call x1, Pallas kernels, body(): pl.pallas_call(functools.partial(layer_kernel, n, cap), out_shape=pltpu.V...  65.3 us

profile of v4, /device:TPU:10, one launch (start us, length us, event | category | flops | bytes accessed | tf_op | source)
XLA Modules:
  0.0 66.0 jit_solution(16433669320398277989)
XLA Ops:
  0.0 65.3 %shard_map.136 = bf16[64,2048]{1,0:T(8,128)(2,1)S(1)} custom-call(bf16[128,1024]{1,0:T(8,128)(2,1)} %query_h.1, bf16[128,1024]{1,0:T(8,128)(2,1)} %logit_h.1, bf16[128,1024]{1,0:T(8,128)(2,1)} %value_h.1, bf16[128,1024]{1,0:T(8,128)(2,1)} %gate_h.1, f32[1,1024]{1,0:T(1,128)} %bitcast.6, f32[1,1024]{1,0:T(1,128)} %bitcast.7, bf16[64,2048]{1,0:T(8,128)(2,1)} %residual_h.1, ...), custom_call_target="tpu_custom_call" | custom-call | tf_op jit(solution)/shard_map/pallas_call | solution.py:706
  65.3 0.7 %copy.16 = bf16[64,2048]{1,0:T(8,128)(2,1)} copy(bf16[64,2048]{1,0:T(8,128)(2,1)S(1)} %shard_map.136) | data formatting | bytes 524288
